TPU v7x, 512 devices: a whole 4x4x16 slice. The times are simulated.
512 devices in a mesh: sp: 32 (over z, core), tp: 16 (over y, x).
Axes of the slice: x: 4, y: 4, z: 16, core: 2. Of those that a mesh axis runs over, the one named last changes fastest.
Arguments:
- residual: bfloat16 [6144, 2048], P('sp'), may hold values from -6 to 6
- query_in: bfloat16 [6144, 2048], P('sp', 'tp'), may hold values from -6 to 6
- value_in: bfloat16 [6144, 2048], P('sp', 'tp'), may hold values from -6 to 6
- forget_fwd: bfloat16 [6144, 2048], P('sp', 'tp'), may hold values from -4.5 to 4.5
- forget_bwd: bfloat16 [6144, 2048], P('sp', 'tp'), may hold values from -4.5 to 4.5
- jumps: float32 [16, 6144], P('tp', 'sp'), may hold values from -2.8 to 0
- gate_gap: float32 [2, 2048], P(None, 'tp'), may hold values from 0 to 0.1
- out_gate: bfloat16 [6144, 2048], P('sp', 'tp'), may hold values from -6 to 6
- head_gain: float32 [2048], P('tp'), may hold values from 0.1 to 1.9
- out_weight: bfloat16 [2048, 2048], P('tp'), may hold values from -0.25 to 0.25
- norm_gain: float32 [2048], replicated, may hold values from 0.1 to 1.9
- route_ids: int32 [6144, 4], P('sp'), may hold values from 0 to 31, all different within a row; in each aligned block of 192 rows (0 to 191, 192 to 383, ...) at most 36 rows name the same one
- route_weights: float32 [6144, 4], P('sp'), may hold values from 0.05 to 0.5
- w_gate: bfloat16 [32, 2048, 4096], P('sp', None, 'tp'), may hold values from -0.375 to 0.375
- w_up: bfloat16 [32, 2048, 4096], P('sp', None, 'tp'), may hold values from -0.375 to 0.375
- w_down: bfloat16 [32, 4096, 2048], P('sp', None, 'tp'), may hold values from -0.09375 to 0.09375
Outputs:
- mixed: bfloat16 [6144, 2048], P('sp', 'tp')
Inputs may be any that keep to these rules, and one draw needn't show every extreme that they name: `route_ids`: in each aligned block of 192 rows each expert is named by at most 36 rows, and by exactly 36 in some block; each row names 4 different experts.
All inputs are finite; a program needn't handle non-finite values.
Results may differ from a plain program's by a relative error of at most 0.024.
Values may be sent and summed in bfloat16 or wider, within the bound.
A program may use at most 64 MiB of HBM per device.

v0:
```python
import math
import jax
import jax.numpy as jnp
from jax import lax
from jax.sharding import Mesh
from jax.sharding import PartitionSpec as P

EXPERTS = 32
CAP = 36
SP = ("sp_0", "sp_1")
highest_precision = lax.Precision.HIGHEST
eps_norm = 1e-06
limit_value = 7.0
alpha_value = 1.702


def filled_with(x, identity):
    return jax.tree.map(
        lambda a, e: jnp.broadcast_to(jnp.asarray(e, a.dtype), a.shape), x, identity
    )


def all_in_one(x, axis):
    leaves = jax.tree.leaves(x)
    turns = sorted(range(len(leaves)), key=lambda k: -leaves[k].size)
    width = (1, *leaves[turns[0]].shape)[-1]
    lines = [
        jnp.pad(leaves[k].reshape(-1), (0, -leaves[k].size % width)).reshape(-1, width)
        for k in turns
    ]
    both, at, found = (lax.all_gather(jnp.concatenate(lines), axis), 0, {})
    for k, line in zip(turns, lines):
        section = both[:, at : at + len(line)].reshape(len(both), -1)
        found[k] = section[:, : leaves[k].size].reshape(-1, *leaves[k].shape)
        at += len(line)
    numbers = iter(range(len(leaves)))
    return jax.tree.map(lambda _: found[next(numbers)], x)


def entering(x, axes, combine, identity, reverse):
    before = start = filled_with(x, identity)
    running = x
    for axis in reversed(axes):
        length, index = (lax.axis_size(axis), lax.axis_index(axis))
        pieces = all_in_one(
            jax.tree.map(
                lambda part, kind: part.astype(kind),
                running,
                jax.tree.map(lambda a: jnp.bfloat16 if a.dtype == jnp.float32 else a.dtype, x),
            ),
            axis,
        )
        inside, running = (start, start)
        for k in reversed(range(length)) if reverse else range(length):
            passed = k > index if reverse else k < index
            running = combine(
                running, jax.tree.map(lambda part, own: part[k].astype(own.dtype), pieces, x)
            )
            inside = jax.tree.map(lambda new, old: jnp.where(passed, new, old), running, inside)
        before = combine(inside, before)
    return before


def in_blocks(x, dim, length):
    shape = x.shape
    pieces = x.reshape(*shape[:dim], length, shape[dim] // length, *shape[dim + 1 :])
    return jnp.moveaxis(pieces, dim, 0)


def sent_and_summed(x, axis, dim):
    length = lax.axis_size(axis)
    pieces = lax.all_to_all(in_blocks(x, dim, length), axis, 0, 0, tiled=True)
    return jnp.sum(pieces.astype(jnp.float32), axis=0)


def rows_for(lines, length):
    spare = -lines.shape[0] % length
    if not spare:
        return lines
    return jnp.concatenate([lines, jnp.zeros((spare, *lines.shape[1:]), lines.dtype)])


def in_order(pieces, dim):
    pieces = jnp.moveaxis(pieces, 0, dim)
    shape = pieces.shape
    return pieces.reshape(*shape[:dim], shape[dim] * shape[dim + 1], *shape[dim + 2 :])


def sent_to_all(x, axis):
    copies = jnp.broadcast_to(x, (lax.axis_size(axis), *x.shape))
    return lax.all_to_all(copies, axis, split_axis=0, concat_axis=0, tiled=True)


def gather_directly(x, axis, dim):
    return in_order(sent_to_all(x, axis), dim)


def sum_by_parts(x, axes):
    lines = x.reshape(-1, x.shape[-1])
    own = sent_and_summed(rows_for(lines, lax.axis_size(axes)), axes, 0)
    whole = gather_directly(own.astype(jnp.bfloat16), axes, 0)
    return whole[: len(lines)].reshape(x.shape).astype(jnp.float32)


def turned_blocks(pieces, axes, turns):
    inside = pieces.shape[1:]
    filled = pieces.reshape(*(lax.axis_size(a) for a in axes), *inside)
    for k in turns:
        filled = lax.all_to_all(filled, axes[k], k, k, tiled=True)
    return filled.reshape(-1, *inside)


def core_and_chips(x, groups, turns, split_dim, concat_dim):
    length = lax.axis_size(groups[0]) * lax.axis_size(groups[1])
    pieces = in_blocks(x, split_dim, length)
    return in_order(turned_blocks(pieces, groups, turns), concat_dim)


def block_pass(queries, keys_in, values, logs):
    head_rows, head_count, head_width = queries.shape
    block_size = math.gcd(head_rows, 64)
    block_count = head_rows // block_size

    def to_blocks(array):
        return array.reshape(block_count, block_size, head_count, array.shape[-1])

    q_block, k_block, v_block, log_block = (
        to_blocks(queries),
        to_blocks(keys_in),
        to_blocks(values),
        to_blocks(logs),
    )
    decay_sums = jnp.cumsum(log_block, axis=1)
    middle = decay_sums[:, block_size // 2 - 1 : block_size // 2]
    scores = jnp.einsum(
        "nthk,nshk->nhts",
        q_block * jnp.exp(decay_sums - middle),
        k_block * jnp.exp(middle - decay_sums),
        precision=highest_precision,
    )
    lower_mask = jnp.tril(jnp.ones((block_size, block_size), bool))
    within = jnp.einsum(
        "nhts,nshv->nthv", jnp.where(lower_mask, scores, 0.0), v_block, precision=highest_precision
    )
    block_end = decay_sums[:, -1]
    q_start = q_block * jnp.exp(decay_sums)
    k_end = k_block * jnp.exp(block_end[:, None] - decay_sums)

    def advance(current_state, block_items):
        query_segment, key_segment, value_segment, decay_part = block_items
        state_readout = jnp.einsum(
            "qwe,wei->qwi", query_segment, current_state, precision=highest_precision
        )
        current_state = current_state * jnp.exp(decay_part)[:, :, None] + jnp.einsum(
            "foj,fox->ojx", key_segment, value_segment, precision=highest_precision
        )
        return (current_state, state_readout)

    zero_state = jnp.zeros((head_count, head_width, values.shape[-1]), jnp.float32)
    final_state, across = lax.scan(advance, zero_state, (q_start, k_end, v_block, block_end))
    return ((within + across).reshape(head_rows, head_count, -1), final_state)


def combine_states(first_part, second_part):
    return (
        first_part[0] * second_part[0],
        second_part[0][:, :, None] * first_part[1] + second_part[1],
    )


def carried(queries, logs, running_state):
    decayed_state = queries * jnp.exp(jnp.cumsum(logs, axis=0))
    return jnp.einsum("una,nae->une", decayed_state, running_state, precision=highest_precision)


def shards(
    residual,
    query_in,
    value_in,
    forget_fwd,
    forget_bwd,
    jumps,
    gate_gap,
    out_gate,
    head_gain,
    out_weight,
    norm_gain,
    route_ids,
    route_weights,
    w_gate,
    w_up,
    w_down,
):
    head_rows, local_width = query_in.shape
    head_count = jumps.shape[0]
    head_width = local_width // head_count

    def by_head(array):
        return array.astype(jnp.float32).reshape(head_rows, head_count, head_width)

    queries = jax.nn.silu(by_head(query_in))
    values = by_head(value_in)
    jump_rows = jnp.transpose(jumps)[:, :, None]

    def gate_terms(forget_in, gap):
        key_share = gap.reshape(head_count, head_width) * jax.nn.sigmoid(-by_head(forget_in))
        return (key_share, jnp.log1p(-key_share) + jump_rows)

    keys_fwd, logs_fwd = gate_terms(forget_fwd, gate_gap[0])
    keys_bwd, logs_bwd = gate_terms(forget_bwd, gate_gap[1])
    ones_part = jnp.ones((head_count, head_width), jnp.float32)
    zero_part = jnp.zeros((head_count, head_width, head_width), jnp.float32)
    local_fwd, final_fwd = block_pass(queries, keys_fwd, values, logs_fwd)
    summary_fwd = (jnp.exp(jnp.sum(logs_fwd, axis=0)), final_fwd)
    carry_fwd = entering(summary_fwd, SP, combine_states, (ones_part, zero_part), False)[1]
    flip_queries = jnp.flip(queries, 0)
    flip_logs = jnp.flip(logs_bwd, 0)
    local_bwd, final_bwd = block_pass(
        flip_queries, jnp.flip(keys_bwd, 0), jnp.flip(values, 0), flip_logs
    )
    summary_bwd = (jnp.exp(jnp.sum(logs_bwd, axis=0)), final_bwd)
    carry_bwd = entering(summary_bwd, SP, combine_states, (ones_part, zero_part), True)[1]
    forward_out = local_fwd + carried(queries, logs_fwd, carry_fwd)
    backward_out = jnp.flip(local_bwd + carried(flip_queries, flip_logs, carry_bwd), 0)
    mixed_heads = forward_out + backward_out
    mean_square = jnp.mean(mixed_heads * mixed_heads, axis=-1, keepdims=True)
    normed = (mixed_heads * lax.rsqrt(mean_square + eps_norm)).reshape(head_rows, local_width)
    gated = (normed * head_gain * jax.nn.silu(out_gate.astype(jnp.float32))).astype(jnp.bfloat16)
    head_terms = jnp.dot(gated, out_weight, preferred_element_type=jnp.float32)
    summed = sum_by_parts(head_terms.astype(jnp.bfloat16), "tp")
    stream = (residual.astype(jnp.float32) + summed).astype(jnp.bfloat16)
    stream_f = stream.astype(jnp.float32)
    row_scale = lax.rsqrt(jnp.mean(stream_f * stream_f, axis=-1, keepdims=True) + eps_norm)
    normed_rows = (stream_f * row_scale * norm_gain).astype(jnp.bfloat16)
    top_count = route_ids.shape[1]
    flat_ids = route_ids.reshape(-1)
    one_hot = (flat_ids[:, None] == jnp.arange(EXPERTS, dtype=jnp.int32)[None, :]).astype(jnp.int32)
    slot_rank = jnp.sum((jnp.cumsum(one_hot, axis=0) - 1) * one_hot, axis=1)
    slot_index = flat_ids * CAP + slot_rank
    owner_rows = jnp.arange(head_rows * top_count, dtype=jnp.int32) // top_count
    slot_rows = jnp.full((EXPERTS * CAP,), head_rows, jnp.int32).at[slot_index].set(owner_rows)
    padded_rows = jnp.concatenate(
        [normed_rows, jnp.zeros((1, normed_rows.shape[1]), jnp.bfloat16)], axis=0
    )
    tp_index = lax.axis_index("tp")
    part_width = w_down.shape[2]
    column_rows = lax.dynamic_slice_in_dim(padded_rows, tp_index * part_width, part_width, 1)
    buffer = column_rows[slot_rows].reshape(EXPERTS, CAP, part_width)
    arrived = lax.all_to_all(buffer, SP, split_axis=0, concat_axis=1, tiled=True)
    piece = lax.all_gather(arrived, "tp", axis=2, tiled=True)
    gate_sum = jnp.einsum("esd,edf->esf", piece, w_gate, preferred_element_type=jnp.float32)
    up_sum = jnp.einsum("esd,edf->esf", piece, w_up, preferred_element_type=jnp.float32)
    gate_sum = jnp.minimum(gate_sum, limit_value)
    up_sum = jnp.clip(up_sum, -limit_value, limit_value)
    active = (gate_sum * jax.nn.sigmoid(alpha_value * gate_sum) * (up_sum + 1.0)).astype(
        jnp.bfloat16
    )
    produced = jnp.einsum(
        "esf,efd->esd",
        lax.all_gather(active, "tp", axis=2, tiled=True),
        w_down,
        preferred_element_type=jnp.float32,
    ).astype(jnp.bfloat16)
    returned = core_and_chips(produced, ("sp_0", "sp_1"), (1, 0), 1, 0)
    picked = returned.reshape(EXPERTS * CAP, part_width)[slot_index].astype(jnp.float32)
    picked = picked.reshape(head_rows, top_count, part_width)
    moe_out = jnp.sum(picked * route_weights[:, :, None], axis=1)
    own_columns = lax.dynamic_slice_in_dim(stream_f, tp_index * part_width, part_width, 1)
    return (own_columns + moe_out).astype(jnp.bfloat16)


def solution(mesh):
    finer = Mesh(mesh.devices.reshape(16, 2, mesh.shape["tp"]), ("sp_0", "sp_1", "tp"))
    return jax.shard_map(
        shards,
        mesh=finer,
        in_specs=(
            P(SP, None),
            P(SP, "tp"),
            P(SP, "tp"),
            P(SP, "tp"),
            P(SP, "tp"),
            P("tp", SP),
            P(None, "tp"),
            P(SP, "tp"),
            P("tp"),
            P("tp", None),
            P(),
            P(SP, None),
            P(SP, None),
            P(SP, None, "tp"),
            P(SP, None, "tp"),
            P(SP, None, "tp"),
        ),
        out_specs=P(SP, "tp"),
        check_vma=False,
    )
```

profile of v0, /device:TPU:2, one launch (start us, length us, event | category | flops | bytes accessed | tf_op | source)
XLA Modules:
  0.0 397.6 jit_solution(2136767596949991621)
XLA Ops:
  10.9 1.7 while.26
  12.6 1.9 all-gather.5
  15.2 38.4 %all-gather.6 = bf16[16,129,128]{2,1,0:T(8,128)(2,1)S(1)} all-gather(bf16[1,129,128]{2,1,0:T(8,128)(2,1)S(1)} %maximum_bitcast_fusion.1), channel_id=3, replica_groups=mesh['sp_0'=16,'sp_1'=2,'tp'=16] {'sp_0'}, dimensions={0}, use_global_device_ids=true | all-gather | bytes 561408 | tf_op jit(solution)/shard_map/all_gather | solution.py:31
  56.6 1.7 while.27
  58.4 1.9 all-gather.7
  61.0 29.2 %all-gather.8 = bf16[16,129,128]{2,1,0:T(8,128)(2,1)S(1)} all-gather(bf16[1,129,128]{2,1,0:T(8,128)(2,1)S(1)} %maximum_bitcast_fusion.3), channel_id=5, replica_groups=mesh['sp_0'=16,'sp_1'=2,'tp'=16] {'sp_0'}, dimensions={0}, use_global_device_ids=true | all-gather | bytes 561408 | tf_op jit(solution)/shard_map/all_gather | solution.py:31
  99.3 7.5 %all-to-all-start = ((bf16[16,12,2048]{2,1,0:T(8,128)(2,1)}), bf16[16,12,2048]{2,1,0:T(8,128)(2,1)S(1)}, u32[]{:S(2)}, u32[]{:S(2)}) async-start(bf16[16,12,2048]{2,1,0:T(8,128)(2,1)} %reshape.1657), calls=%async_computation | async-start | bytes 2097152 | tf_op jit(solution)/shard_map/all_to_all | solution.py:72
  107.0 1.7 reduce-window.26
  108.7 9.9 %all-to-all-done = bf16[16,12,2048]{2,1,0:T(8,128)(2,1)S(1)} async-done(((bf16[16,12,2048]{2,1,0:T(8,128)(2,1)}), bf16[16,12,2048]{2,1,0:T(8,128)(2,1)S(1)}, u32[]{:S(2)}, u32[]{:S(2)}) %all-to-all-start) | async-done | bytes 786464 | tf_op jit(solution)/shard_map/all_to_all | solution.py:72
  120.0 5.0 %all-to-all-start.1 = ((bf16[16,12,2048]{2,1,0:T(8,128)(2,1)}), bf16[16,12,2048]{2,1,0:T(8,128)(2,1)S(1)}, u32[]{:S(2)}, u32[]{:S(2)}) async-start(bf16[16,12,2048]{2,1,0:T(8,128)(2,1)} %broadcast_in_dim.35), calls=%async_computation.1 | async-start | bytes 2097152 | tf_op jit(solution)/shard_map/all_to_all | solution.py:91
  125.7 3.4 scatter_custom_fusion
  129.2 7.8 %all-to-all-done.1 = bf16[16,12,2048]{2,1,0:T(8,128)(2,1)S(1)} async-done(((bf16[16,12,2048]{2,1,0:T(8,128)(2,1)}), bf16[16,12,2048]{2,1,0:T(8,128)(2,1)S(1)}, u32[]{:S(2)}, u32[]{:S(2)}) %all-to-all-start.1) | async-done | bytes 786464 | tf_op jit(solution)/shard_map/all_to_all | solution.py:91
  138.3 1.7 multiply_reduce_fusion
  140.2 2.9 gather_fusion
  143.2 33.2 %all_to_all.32 = bf16[32,36,128]{2,1,0:T(8,128)(2,1)S(1)} all-to-all(bf16[32,36,128]{2,1,0:T(8,128)(2,1)S(1)} %reshape.1659), channel_id=1, replica_groups=mesh['sp_0'=16,'sp_1'=2,'tp'=16] {'sp_0','sp_1'}, dimensions={0} | all-to-all | bytes 589824 | tf_op jit(solution)/shard_map/all_to_all | solution.py:249
  177.5 62.6 %all-gather.12.cloned.1.call-done = bf16[1,1152,2048]{2,1,0:T(8,128)(2,1)} async-done(((bf16[1,1152,128]{2,1,0:T(8,128)(2,1)}), bf16[1,1152,2048]{2,1,0:T(8,128)(2,1)}) %all-gather.12.cloned.1.call-update) | async-done | bytes 4718608 | tf_op jit(solution)/shard_map/all_gather | solution.py:250
  240.1 3.9 fusion.25
  244.1 2.4 fusion.34
  246.6 97.4 %all-gather.14.cloned.1.call-done = bf16[1152,4096]{1,0:T(8,128)(2,1)} async-done(((bf16[1152,256]{1,0:T(8,128)(2,1)}), bf16[1152,4096]{1,0:T(8,128)(2,1)}) %all-gather.14.cloned.1.call-update) | async-done | bytes 9437200 | tf_op jit(solution)/shard_map/all_gather | solution.py:260
  344.0 6.5 %convolution_convert_fusion.1 = bf16[1152,128]{1,0:T(8,128)(2,1)S(1)} fusion(bf16[1152,4096]{1,0:T(8,128)(2,1)} %all-gather.14.cloned.1.call-done, bf16[1,4096,128]{2,1,0:T(8,128)(2,1)} %param.35), kind=kOutput, calls=%fused_computation.43 | convolution fusion | flops 1208107008 | bytes 10780672 | tf_op jit(solution)/shard_map/esf,efd->esd/dot_general | solution.py:258
  350.7 4.0 all_to_all.33
  355.6 12.3 %all-to-all-start.4 = ((bf16[16,2,1,36,128]{4,1,3,2,0:T(2,128)(2,1)}), bf16[16,2,1,36,128]{4,1,3,2,0:T(2,128)(2,1)S(1)}, u32[]{:S(2)}, u32[]{:S(2)}) async-start(bf16[16,2,1,36,128]{4,1,3,2,0:T(2,128)(2,1)} %copy.64), calls=%async_computation.4 | async-start | bytes 589824 | tf_op jit(solution)/shard_map/all_to_all | solution.py:109
  368.1 19.8 %all-to-all-done.4 = bf16[16,2,1,36,128]{4,1,3,2,0:T(2,128)(2,1)S(1)} async-done(((bf16[16,2,1,36,128]{4,1,3,2,0:T(2,128)(2,1)}), bf16[16,2,1,36,128]{4,1,3,2,0:T(2,128)(2,1)S(1)}, u32[]{:S(2)}, u32[]{:S(2)}) %all-to-all-start.4) | async-done | bytes 294944 | tf_op jit(solution)/shard_map/all_to_all | solution.py:109
  387.9 1.9 gather_fusion.1
  (212 shorter events, 27.7 us)
Async XLA Ops:
  6.5 233.5 %copy-start = (bf16[1,2048,256]{2,1,0:T(8,128)(2,1)S(1)}, bf16[1,2048,256]{2,1,0:T(8,128)(2,1)}, u32[]{:S(2)}) copy-start(bf16[1,2048,256]{2,1,0:T(8,128)(2,1)} %param.33) | copy-start | bytes 3145732
  10.9 44.1 %copy-start.3 = (bf16[192,128]{1,0:T(8,128)(2,1)S(1)}, bf16[192,128]{1,0:T(8,128)(2,1)}, u32[]{:S(2)}) copy-start(bf16[192,128]{1,0:T(8,128)(2,1)} %param.22) | copy-start | bytes 147460
  12.6 41.7 %copy-start.4 = (f32[3,64,1,128]{3,1,2,0:T(8,128)}, f32[3,64,1,128]{3,1,2,0:T(8,128)S(1)}, u32[]{:S(2)}) copy-start(f32[3,64,1,128]{3,1,2,0:T(8,128)S(1)} %get-tuple-element.81) | copy-start | bytes 294916
  14.5 40.9 %copy-start.7 = (bf16[2,129,128]{2,1,0:T(8,128)(2,1)}, bf16[2,129,128]{2,1,0:T(8,128)(2,1)S(1)}, u32[]{:S(2)}) copy-start(bf16[2,129,128]{2,1,0:T(8,128)(2,1)S(1)} %all-gather.5) | copy-start | bytes 198148
  14.5 40.9 %copy-start.19 = (f32[128]{0:T(128)}, f32[128]{0:T(128)S(1)}, u32[]{:S(2)}) copy-start(f32[128]{0:T(128)S(1)} %fusion.382) | copy-start | bytes 1540
  15.1 40.3 %copy-start.16 = (f32[128]{0:T(128)}, f32[128]{0:T(128)S(1)}, u32[]{:S(2)}) copy-start(f32[128]{0:T(128)S(1)} %get-tuple-element.212) | copy-start | bytes 1540
  58.3 2.6 copy-start.6
  58.3 33.5 %copy-start.12 = (f32[3,128]{1,0:T(4,128)S(1)}, f32[3,128]{1,0:T(4,128)}, u32[]{:S(2)}) copy-start(f32[3,128]{1,0:T(4,128)} %get-tuple-element.225) | copy-start | bytes 4612
  60.2 31.1 %copy-start.8 = (bf16[2,129,128]{2,1,0:T(8,128)(2,1)}, bf16[2,129,128]{2,1,0:T(8,128)(2,1)S(1)}, u32[]{:S(2)}) copy-start(bf16[2,129,128]{2,1,0:T(8,128)(2,1)S(1)} %all-gather.7) | copy-start | bytes 198148
  92.1 3.2 copy-start.11
  93.3 2.6 copy-start.10
  93.3 2.6 copy-start.17
  93.3 2.6 copy-start.20
  93.3 2.6 copy-start.21
  98.1 8.7 %copy-start.13 = (s32[192,4]{0,1:T(4,128)S(1)}, s32[192,4]{0,1:T(4,128)}, u32[]{:S(2)}) copy-start(s32[192,4]{0,1:T(4,128)} %param.31) | copy-start | bytes 9220
  99.3 19.4 %all-to-all-start = ((bf16[16,12,2048]{2,1,0:T(8,128)(2,1)}), bf16[16,12,2048]{2,1,0:T(8,128)(2,1)S(1)}, u32[]{:S(2)}, u32[]{:S(2)}) async-start(bf16[16,12,2048]{2,1,0:T(8,128)(2,1)} %reshape.1657), calls=%async_computation | async-start | bytes 2097152 | tf_op jit(solution)/shard_map/all_to_all | solution.py:72
  120.0 17.0 %all-to-all-start.1 = ((bf16[16,12,2048]{2,1,0:T(8,128)(2,1)}), bf16[16,12,2048]{2,1,0:T(8,128)(2,1)S(1)}, u32[]{:S(2)}, u32[]{:S(2)}) async-start(bf16[16,12,2048]{2,1,0:T(8,128)(2,1)} %broadcast_in_dim.35), calls=%async_computation.1 | async-start | bytes 2097152 | tf_op jit(solution)/shard_map/all_to_all | solution.py:91
  124.9 115.1 %all-gather.12.cloned.1.call-start = ((), (), s32[]{:S(2)}) async-start(), calls=%async_computation.5 | async-start | bytes 5013504 | tf_op jit(solution)/shard_map/all_gather | solution.py:250
  125.2 13.1 %copy-start.1 = (bf16[192,2048]{1,0:T(8,128)(2,1)S(1)}, bf16[192,2048]{1,0:T(8,128)(2,1)}, u32[]{:S(2)}) copy-start(bf16[192,2048]{1,0:T(8,128)(2,1)} %param.20) | copy-start | bytes 2359300
  177.3 166.7 %all-gather.14.cloned.1.call-start = ((), (), s32[]{:S(2)}) async-start(), calls=%async_computation.6 | async-start | bytes 10027008 | tf_op jit(solution)/shard_map/all_gather | solution.py:260
  240.1 3.9 copy-start.37
  240.1 4.1 %copy-start.38 = (bf16[1,2048,256]{2,1,0:T(8,128)(2,1)S(1)}, bf16[1,2048,256]{2,1,0:T(8,128)(2,1)}, u32[]{:S(2)}) copy-start(bf16[1,2048,256]{2,1,0:T(8,128)(2,1)} %param.34) | copy-start | bytes 3145732
  350.5 17.4 %copy-start.15 = (f32[192,4]{0,1:T(4,128)S(1)}, f32[192,4]{0,1:T(4,128)}, u32[]{:S(2)}) copy-start(f32[192,4]{0,1:T(4,128)} %param.32) | copy-start | bytes 9220
  355.6 32.2 %all-to-all-start.4 = ((bf16[16,2,1,36,128]{4,1,3,2,0:T(2,128)(2,1)}), bf16[16,2,1,36,128]{4,1,3,2,0:T(2,128)(2,1)S(1)}, u32[]{:S(2)}, u32[]{:S(2)}) async-start(bf16[16,2,1,36,128]{4,1,3,2,0:T(2,128)(2,1)} %copy.64), calls=%async_computation.4 | async-start | bytes 589824 | tf_op jit(solution)/shard_map/all_to_all | solution.py:109
  (21 other events, 51.9 us)
Sparse Core Ops, SparseCore 0:
  177.4 62.6 all-gather.11
  246.7 97.2 all-gather.13
where the time goes:
time: 398 us
  waiting for transfers between devices  197 us (49%)
  blocking collectives  108 us (27%)
  starting transfers between devices  25 us (6%)
  matrix products  21.1 us (5%)
  local copies, waits for them, and re-layouts  18.4 us (5%)
  between operations  14.5 us (4%)
  other arithmetic  12.4 us (3%)
    all_gather x1, waiting for transfers between devices, shards(): lax.all_gather(active, 'tp', axis=2, tiled=True)  97.4 us
    all_gather x4, blocking collectives, all_in_one(): both, at, found = (lax.all_gather(jnp.concatenate(lines), axis), 0, {})  71.3 us
    all_gather x1, waiting for transfers between devices, shards(): piece = lax.all_gather(arrived, 'tp', axis=2, tiled=True)  62.6 us
    all_to_all x1, blocking collectives, shards(): lax.all_to_all(buffer, SP, split_axis=0, concat_axis=1, tiled=True)  33.2 us
    all_to_all x1, waiting for transfers between devices, turned_blocks(): filled = lax.all_to_all(filled, axes[k], k, k, tiled=True)  19.8 us
    all_to_all x1, starting transfers between devices, turned_blocks(): filled = lax.all_to_all(filled, axes[k], k, k, tiled=True)  12.3 us
    all_to_all x1, waiting for transfers between devices, sent_and_summed(): pieces = lax.all_to_all(in_blocks(x, dim, length), axis, 0, 0, tiled=True)  9.91 us
  transfers between devices with their start and end apart: 5, of which 5 were waited for; matrix products, arithmetic and copies ran while one was open for 2% of the time, Pallas kernels for 0%

commit v1 on v0

--- a/solution.py
+++ b/solution.py
@@ -247,7 +247,9 @@
     column_rows = lax.dynamic_slice_in_dim(padded_rows, tp_index * part_width, part_width, 1)
     buffer = column_rows[slot_rows].reshape(EXPERTS, CAP, part_width)
     arrived = lax.all_to_all(buffer, SP, split_axis=0, concat_axis=1, tiled=True)
-    piece = lax.all_gather(arrived, "tp", axis=2, tiled=True)
+    piece = jnp.concatenate(
+        lax.all_to_all(jnp.stack([arrived] * lax.axis_size("tp")), "tp", 0, 0), axis=2
+    )
     gate_sum = jnp.einsum("esd,edf->esf", piece, w_gate, preferred_element_type=jnp.float32)
     up_sum = jnp.einsum("esd,edf->esf", piece, w_up, preferred_element_type=jnp.float32)
     gate_sum = jnp.minimum(gate_sum, limit_value)

time: 398 us -> 386 us (0.970)
  waiting for transfers between devices: 197 us -> 126 us
  blocking collectives: 108 us -> 168 us
    all_gather x1 -> x0, waiting for transfers between devices: 62.6 us -> none  [shards(): piece = lax.all_gather(arrived, 'tp', axis=2, tiled=True)]
    all_to_all x0 -> x1, blocking collectives: none -> 59.4 us  [shards(): lax.all_to_all(jnp.stack([arrived] * lax.axis_size('tp')), 'tp', 0, 0)]
    all_gather x1, waiting for transfers between devices: 97.4 us -> 88.5 us  [shards(): lax.all_gather(active, 'tp', axis=2, tiled=True)]
  transfers between devices with their start and end apart: 5 -> 4, of which waited for: 5 -> 4; matrix products, arithmetic and copies ran while one was open for 2% -> 2% of each run, Pallas kernels for 0% -> 0%
where the time goes in v1:
time: 386 us; the launch traced here: 385 us
  blocking collectives  168 us (44%)
  waiting for transfers between devices  126 us (33%)
  starting transfers between devices  24.8 us (6%)
  local copies, waits for them, and re-layouts  20.1 us (5%)
  matrix products  18.5 us (5%)
  between operations  14.7 us (4%)
  other arithmetic  12.5 us (3%)
    all_gather x1, waiting for transfers between devices, shards(): lax.all_gather(active, 'tp', axis=2, tiled=True)  88.5 us
    all_gather x4, blocking collectives, all_in_one(): both, at, found = (lax.all_gather(jnp.concatenate(lines), axis), 0, {})  71.3 us
    all_to_all x1, blocking collectives, shards(): lax.all_to_all(jnp.stack([arrived] * lax.axis_size('tp')), 'tp', 0, 0)  59.4 us
    all_to_all x1, blocking collectives, shards(): lax.all_to_all(buffer, SP, split_axis=0, concat_axis=1, tiled=True)  33.2 us
    all_to_all x1, waiting for transfers between devices, turned_blocks(): filled = lax.all_to_all(filled, axes[k], k, k, tiled=True)  19.8 us
    all_to_all x1, starting transfers between devices, turned_blocks(): filled = lax.all_to_all(filled, axes[k], k, k, tiled=True)  12.3 us
    all_to_all x1, waiting for transfers between devices, sent_and_summed(): pieces = lax.all_to_all(in_blocks(x, dim, length), axis, 0, 0, tiled=True)  9.91 us
    all_to_all x1, waiting for transfers between devices, sent_to_all(): return lax.all_to_all(copies, axis, split_axis=0, concat_axis=0, tiled=True)  7.78 us
  transfers between devices with their start and end apart: 4, of which 4 were waited for; matrix products, arithmetic and copies ran while one was open for 2% of the time, Pallas kernels for 0%

profile of v1, /device:TPU:2, one launch (start us, length us, event | category | flops | bytes accessed | tf_op | source)
XLA Modules:
  0.0 384.8 jit_solution(6561677924764157860)
XLA Ops:
  10.9 1.7 while.26
  12.7 1.9 all-gather.5
  15.2 38.4 %all-gather.6 = bf16[16,129,128]{2,1,0:T(8,128)(2,1)S(1)} all-gather(bf16[1,129,128]{2,1,0:T(8,128)(2,1)S(1)} %maximum_bitcast_fusion.1), channel_id=3, replica_groups=mesh['sp_0'=16,'sp_1'=2,'tp'=16] {'sp_0'}, dimensions={0}, use_global_device_ids=true | all-gather | bytes 561408 | tf_op jit(solution)/shard_map/all_gather | solution.py:31
  56.5 1.7 while.27
  58.3 1.9 all-gather.7
  60.9 29.2 %all-gather.8 = bf16[16,129,128]{2,1,0:T(8,128)(2,1)S(1)} all-gather(bf16[1,129,128]{2,1,0:T(8,128)(2,1)S(1)} %maximum_bitcast_fusion.3), channel_id=5, replica_groups=mesh['sp_0'=16,'sp_1'=2,'tp'=16] {'sp_0'}, dimensions={0}, use_global_device_ids=true | all-gather | bytes 561408 | tf_op jit(solution)/shard_map/all_gather | solution.py:31
  96.1 1.6 multiply_reduce_fusion.1
  99.4 7.5 %all-to-all-start = ((bf16[16,12,2048]{2,1,0:T(8,128)(2,1)}), bf16[16,12,2048]{2,1,0:T(8,128)(2,1)S(1)}, u32[]{:S(2)}, u32[]{:S(2)}) async-start(bf16[16,12,2048]{2,1,0:T(8,128)(2,1)} %reshape.1668), calls=%async_computation | async-start | bytes 2097152 | tf_op jit(solution)/shard_map/all_to_all | solution.py:72
  107.1 1.7 reduce-window.26
  108.8 9.9 %all-to-all-done = bf16[16,12,2048]{2,1,0:T(8,128)(2,1)S(1)} async-done(((bf16[16,12,2048]{2,1,0:T(8,128)(2,1)}), bf16[16,12,2048]{2,1,0:T(8,128)(2,1)S(1)}, u32[]{:S(2)}, u32[]{:S(2)}) %all-to-all-start) | async-done | bytes 786464 | tf_op jit(solution)/shard_map/all_to_all | solution.py:72
  120.1 5.0 %all-to-all-start.1 = ((bf16[16,12,2048]{2,1,0:T(8,128)(2,1)}), bf16[16,12,2048]{2,1,0:T(8,128)(2,1)S(1)}, u32[]{:S(2)}, u32[]{:S(2)}) async-start(bf16[16,12,2048]{2,1,0:T(8,128)(2,1)} %broadcast_in_dim.35), calls=%async_computation.1 | async-start | bytes 2097152 | tf_op jit(solution)/shard_map/all_to_all | solution.py:91
  125.8 3.4 scatter_custom_fusion
  129.3 7.8 %all-to-all-done.1 = bf16[16,12,2048]{2,1,0:T(8,128)(2,1)S(1)} async-done(((bf16[16,12,2048]{2,1,0:T(8,128)(2,1)}), bf16[16,12,2048]{2,1,0:T(8,128)(2,1)S(1)}, u32[]{:S(2)}, u32[]{:S(2)}) %all-to-all-start.1) | async-done | bytes 786464 | tf_op jit(solution)/shard_map/all_to_all | solution.py:91
  138.4 1.9 multiply_reduce_fusion
  140.5 2.9 gather_fusion
  143.5 33.2 %all_to_all.34 = bf16[32,36,128]{2,1,0:T(8,128)(2,1)S(1)} all-to-all(bf16[32,36,128]{2,1,0:T(8,128)(2,1)S(1)} %reshape.1670), channel_id=1, replica_groups=mesh['sp_0'=16,'sp_1'=2,'tp'=16] {'sp_0','sp_1'}, dimensions={0} | all-to-all | bytes 589824 | tf_op jit(solution)/shard_map/all_to_all | solution.py:249
  179.3 59.4 %all_to_all.35 = bf16[16,1,1152,128]{2,3,1,0:T(8,128)(2,1)S(1)} all-to-all(bf16[16,1,1152,128]{2,3,1,0:T(8,128)(2,1)S(1)} %stack.5), channel_id=1, replica_groups=mesh['sp_0'=16,'sp_1'=2,'tp'=16] {'tp'}, dimensions={0} | all-to-all | bytes 9437184 | tf_op jit(solution)/shard_map/all_to_all | solution.py:251
  240.2 2.4 fusion.20
  242.6 88.5 %all-gather.11.cloned.1.call-done = bf16[1152,4096]{1,0:T(8,128)(2,1)} async-done(((bf16[1152,256]{1,0:T(8,128)(2,1)}), bf16[1152,4096]{1,0:T(8,128)(2,1)}) %all-gather.11.cloned.1.call-update) | async-done | bytes 9437200 | tf_op jit(solution)/shard_map/all_gather | solution.py:262
  331.2 6.5 %convolution_convert_fusion.1 = bf16[1152,128]{1,0:T(8,128)(2,1)S(1)} fusion(bf16[1152,4096]{1,0:T(8,128)(2,1)} %all-gather.11.cloned.1.call-done, bf16[1,4096,128]{2,1,0:T(8,128)(2,1)} %param.35), kind=kOutput, calls=%fused_computation.39 | convolution fusion | flops 1208107008 | bytes 10780672 | tf_op jit(solution)/shard_map/esf,efd->esd/dot_general | solution.py:260
  337.8 4.0 %all_to_all.36 = bf16[16,2,1,36,128]{4,0,3,2,1:T(8,128)(2,1)S(1)} all-to-all(bf16[16,2,1,36,128]{4,0,3,2,1:T(8,128)(2,1)S(1)} %copy.66), channel_id=1, replica_groups=mesh['sp_0'=16,'sp_1'=2,'tp'=16] {'sp_1'}, dimensions={1} | all-to-all | bytes 589824 | tf_op jit(solution)/shard_map/all_to_all | solution.py:109
  342.8 12.3 %all-to-all-start.5 = ((bf16[16,2,1,36,128]{4,1,3,2,0:T(2,128)(2,1)}), bf16[16,2,1,36,128]{4,1,3,2,0:T(2,128)(2,1)S(1)}, u32[]{:S(2)}, u32[]{:S(2)}) async-start(bf16[16,2,1,36,128]{4,1,3,2,0:T(2,128)(2,1)} %copy.67), calls=%async_computation.5 | async-start | bytes 589824 | tf_op jit(solution)/shard_map/all_to_all | solution.py:109
  355.2 19.8 %all-to-all-done.5 = bf16[16,2,1,36,128]{4,1,3,2,0:T(2,128)(2,1)S(1)} async-done(((bf16[16,2,1,36,128]{4,1,3,2,0:T(2,128)(2,1)}), bf16[16,2,1,36,128]{4,1,3,2,0:T(2,128)(2,1)S(1)}, u32[]{:S(2)}, u32[]{:S(2)}) %all-to-all-start.5) | async-done | bytes 294944 | tf_op jit(solution)/shard_map/all_to_all | solution.py:109
  375.1 1.9 gather_fusion.1
  (226 shorter events, 28.9 us)
Async XLA Ops:
  6.5 232.2 %copy-start = (bf16[1,2048,256]{2,1,0:T(8,128)(2,1)S(1)}, bf16[1,2048,256]{2,1,0:T(8,128)(2,1)}, u32[]{:S(2)}) copy-start(bf16[1,2048,256]{2,1,0:T(8,128)(2,1)} %param.33) | copy-start | bytes 3145732
  10.9 44.0 %copy-start.2 = (bf16[192,128]{1,0:T(8,128)(2,1)S(1)}, bf16[192,128]{1,0:T(8,128)(2,1)}, u32[]{:S(2)}) copy-start(bf16[192,128]{1,0:T(8,128)(2,1)} %param.22) | copy-start | bytes 147460
  12.6 42.2 %copy-start.3 = (f32[3,64,1,128]{3,1,2,0:T(8,128)}, f32[3,64,1,128]{3,1,2,0:T(8,128)S(1)}, u32[]{:S(2)}) copy-start(f32[3,64,1,128]{3,1,2,0:T(8,128)S(1)} %get-tuple-element.81) | copy-start | bytes 294916
  14.5 40.6 %copy-start.6 = (bf16[2,129,128]{2,1,0:T(8,128)(2,1)}, bf16[2,129,128]{2,1,0:T(8,128)(2,1)S(1)}, u32[]{:S(2)}) copy-start(bf16[2,129,128]{2,1,0:T(8,128)(2,1)S(1)} %all-gather.5) | copy-start | bytes 198148
  14.5 40.6 %copy-start.18 = (f32[128]{0:T(128)}, f32[128]{0:T(128)S(1)}, u32[]{:S(2)}) copy-start(f32[128]{0:T(128)S(1)} %fusion.366) | copy-start | bytes 1540
  15.1 40.0 %copy-start.15 = (f32[128]{0:T(128)}, f32[128]{0:T(128)S(1)}, u32[]{:S(2)}) copy-start(f32[128]{0:T(128)S(1)} %get-tuple-element.212) | copy-start | bytes 1540
  58.2 2.6 copy-start.5
  58.2 33.6 %copy-start.11 = (f32[3,128]{1,0:T(4,128)S(1)}, f32[3,128]{1,0:T(4,128)}, u32[]{:S(2)}) copy-start(f32[3,128]{1,0:T(4,128)} %get-tuple-element.225) | copy-start | bytes 4612
  60.1 31.1 %copy-start.7 = (bf16[2,129,128]{2,1,0:T(8,128)(2,1)}, bf16[2,129,128]{2,1,0:T(8,128)(2,1)S(1)}, u32[]{:S(2)}) copy-start(bf16[2,129,128]{2,1,0:T(8,128)(2,1)S(1)} %all-gather.7) | copy-start | bytes 198148
  92.2 3.2 copy-start.10
  93.4 2.5 copy-start.9
  93.4 2.5 copy-start.16
  93.4 2.5 copy-start.19
  93.5 2.5 copy-start.20
  93.5 2.5 copy-start.21
  93.5 2.5 copy-start.22
  93.5 2.5 copy-start.23
  93.5 2.5 copy-start.24
  98.2 8.7 %copy-start.12 = (s32[192,4]{0,1:T(4,128)S(1)}, s32[192,4]{0,1:T(4,128)}, u32[]{:S(2)}) copy-start(s32[192,4]{0,1:T(4,128)} %param.31) | copy-start | bytes 9220
  99.4 19.4 %all-to-all-start = ((bf16[16,12,2048]{2,1,0:T(8,128)(2,1)}), bf16[16,12,2048]{2,1,0:T(8,128)(2,1)S(1)}, u32[]{:S(2)}, u32[]{:S(2)}) async-start(bf16[16,12,2048]{2,1,0:T(8,128)(2,1)} %reshape.1668), calls=%async_computation | async-start | bytes 2097152 | tf_op jit(solution)/shard_map/all_to_all | solution.py:72
  120.1 17.0 %all-to-all-start.1 = ((bf16[16,12,2048]{2,1,0:T(8,128)(2,1)}), bf16[16,12,2048]{2,1,0:T(8,128)(2,1)S(1)}, u32[]{:S(2)}, u32[]{:S(2)}) async-start(bf16[16,12,2048]{2,1,0:T(8,128)(2,1)} %broadcast_in_dim.35), calls=%async_computation.1 | async-start | bytes 2097152 | tf_op jit(solution)/shard_map/all_to_all | solution.py:91
  125.0 206.1 %all-gather.11.cloned.1.call-start = ((), (), s32[]{:S(2)}) async-start(), calls=%async_computation.6 | async-start | bytes 10027008 | tf_op jit(solution)/shard_map/all_gather | solution.py:262
  337.7 17.4 %copy-start.14 = (f32[192,4]{0,1:T(4,128)S(1)}, f32[192,4]{0,1:T(4,128)}, u32[]{:S(2)}) copy-start(f32[192,4]{0,1:T(4,128)} %param.32) | copy-start | bytes 9220
  342.8 32.2 %all-to-all-start.5 = ((bf16[16,2,1,36,128]{4,1,3,2,0:T(2,128)(2,1)}), bf16[16,2,1,36,128]{4,1,3,2,0:T(2,128)(2,1)S(1)}, u32[]{:S(2)}, u32[]{:S(2)}) async-start(bf16[16,2,1,36,128]{4,1,3,2,0:T(2,128)(2,1)} %copy.67), calls=%async_computation.5 | async-start | bytes 589824 | tf_op jit(solution)/shard_map/all_to_all | solution.py:109
  (27 other events, 59.1 us)
Sparse Core Ops, SparseCore 0:
  242.7 88.3 all-gather.10
